TPU v7x, 32 devices: a whole 2x2x4 slice. The times are simulated.
32 devices in a mesh: ep: 16 (over z, y, x), tp: 2 (over core).
Axes of the slice: x: 2, y: 2, z: 4, core: 2. Of those that a mesh axis runs over, the one named last changes fastest.
Arguments:
- tokens: bfloat16 [256, 2048], P('ep'), may hold values from -6 to 6
- lengths: int32 [256], P('ep'), may hold values from 1024 to 8191
- prior_state: float32 [256, 16, 64, 64], P('ep', 'tp'), may hold values from -2 to 2
- mix_gain: float32 [2048], replicated, may hold values from 0.1 to 1.9
- post_gain: float32 [2048], replicated, may hold values from 0.1 to 1.9
- ffn_gain: float32 [2048], replicated, may hold values from 0.1 to 1.9
- out_gain: float32 [2048], replicated, may hold values from 0.1 to 1.9
- query_weight: bfloat16 [2048, 1024], P('ep', 'tp'), may hold values from -0.125 to 0.125
- key_weight: bfloat16 [2048, 1024], P('ep', 'tp'), may hold values from -0.125 to 0.125
- value_weight: bfloat16 [2048, 1024], P('ep', 'tp'), may hold values from -0.125 to 0.125
- gate_weight: bfloat16 [2048, 1024], P('ep', 'tp'), may hold values from -0.125 to 0.125
- out_weight: bfloat16 [1024, 2048], P('tp', 'ep'), may hold values from -0.1875 to 0.1875
- routes: int32 [256, 6], P('ep'), may hold values from 0 to 15, all different within a row; in each aligned block of 16 rows (0 to 15, 16 to 31, ...) at most 8 rows name the same one
- route_gates: float32 [256, 6], P('ep'), may hold values from 0.1 to 0.9
- expert_gate: bfloat16 [16, 2048, 512], P('ep', None, 'tp'), may hold values from -0.125 to 0.125
- expert_up: bfloat16 [16, 2048, 512], P('ep', None, 'tp'), may hold values from -0.125 to 0.125
- expert_down: bfloat16 [16, 512, 2048], P('ep', 'tp'), may hold values from -0.25 to 0.25
- shared_gate: bfloat16 [2048, 512], P(None, 'tp'), may hold values from -0.125 to 0.125
- shared_up: bfloat16 [2048, 512], P(None, 'tp'), may hold values from -0.125 to 0.125
- shared_down: bfloat16 [512, 2048], P('tp'), may hold values from -0.25 to 0.25
Outputs:
- result: bfloat16 [256, 2048], P('ep')
- new_state: float32 [256, 16, 64, 64], P('ep', 'tp')
Inputs may be any that keep to these rules, and one draw needn't show every extreme that they name: `routes`: each row names 6 different experts. In the rows of one device (aligned blocks of 16 rows) no expert is named more than 8 times, and in every draw some expert is named exactly 8 times in some block.
All inputs are finite; a program needn't handle non-finite values.
Results may differ from a plain program's by a relative error of at most 0.02.
Values may be sent and summed in bfloat16 or wider, within the bound.
A program may use at most 128 MiB of HBM per device.

v0:
```python
import jax
import jax.numpy as jnp
from jax import lax
from jax.sharding import PartitionSpec as P

HEAD = 64
HEADS = 16
EPS = 1e-06
THETA = 10000.0


def rounded(values):
    return lax.optimization_barrier(values.astype(jnp.bfloat16)).astype(jnp.float32)


def scaled_rows(values, gain_row):
    widened = values.astype(jnp.float32)
    return widened * lax.rsqrt(jnp.mean(widened * widened, axis=-1, keepdims=True) + EPS) * gain_row


def rotate(vectors, lengths):
    half_dim = vectors.shape[-1] // 2
    frequency = THETA ** (-jnp.arange(half_dim, dtype=jnp.float32) / half_dim)
    angles = lengths.astype(jnp.float32)[:, None] * frequency[None, :]
    cosine = jnp.cos(angles)[:, None, :]
    sine_part = jnp.sin(angles)[:, None, :]
    leading = vectors[..., :half_dim]
    trailing = vectors[..., half_dim:]
    return jnp.concatenate(
        [leading * cosine - trailing * sine_part, trailing * cosine + leading * sine_part], axis=-1
    )


def decay_table(head_count):
    head_order = jnp.arange(head_count, dtype=jnp.float32)
    return 1.0 - jnp.exp2(-5.0 - 7.0 * head_order / (head_count - 1))


def retain(queries, keys_new, values, out_gate, prior_state, lengths, decays):
    seq_count = queries.shape[0]
    head_count = decays.shape[0]
    layout = (seq_count, head_count, HEAD)
    rot_query = rotate(queries.astype(jnp.float32).reshape(layout), lengths)
    rot_key = rotate(keys_new.astype(jnp.float32).reshape(layout), lengths) * HEAD ** (-0.5)
    wide_values = values.astype(jnp.float32).reshape(layout)
    from_state = jnp.einsum(
        "shd,shde->she", rot_query, prior_state, precision=lax.Precision.HIGHEST
    )
    self_term = jnp.sum(rot_query * rot_key, axis=-1, keepdims=True)
    read_out = decays[None, :, None] * from_state + self_term * wide_values
    new_state = (
        decays[None, :, None, None] * prior_state
        + rot_key[..., :, None] * wide_values[..., None, :]
    )
    normed = read_out * lax.rsqrt(jnp.mean(read_out * read_out, axis=-1, keepdims=True) + EPS)
    gated_rows = normed.reshape(seq_count, head_count * HEAD) * jax.nn.silu(
        out_gate.astype(jnp.float32)
    )
    return (gated_rows.astype(jnp.bfloat16), new_state)


def on_device(
    tokens,
    lengths,
    prior_state,
    mix_gain,
    post_gain,
    ffn_gain,
    out_gain,
    query_weight,
    key_weight,
    value_weight,
    gate_weight,
    out_weight,
    routes,
    route_gates,
    expert_gate,
    expert_up,
    expert_down,
    shared_gate,
    shared_up,
    shared_down,
):
    seq_here = tokens.shape[0]
    model_width = tokens.shape[1]
    local_cols = query_weight.shape[1]
    normed = scaled_rows(tokens, mix_gain).astype(jnp.bfloat16)
    features = lax.all_to_all(normed, "ep", split_axis=1, concat_axis=0, tiled=True)
    joined = jnp.concatenate((query_weight, key_weight, value_weight, gate_weight), axis=1)
    summed = lax.psum_scatter(
        jnp.dot(features, joined, preferred_element_type=jnp.float32),
        "ep",
        scatter_dimension=0,
        tiled=True,
    )
    projected = tuple((summed[:, role * local_cols : (role + 1) * local_cols] for role in range(4)))
    queries, keys_new, values, out_gate = tuple(
        (member.astype(jnp.bfloat16) for member in projected)
    )
    heads_here = local_cols // HEAD
    decays = lax.dynamic_slice_in_dim(
        decay_table(HEADS), lax.axis_index("tp") * heads_here, heads_here, 0
    )
    retained, new_state = retain(queries, keys_new, values, out_gate, prior_state, lengths, decays)
    column_part = jnp.dot(
        lax.all_gather(retained, "ep", axis=0, tiled=True),
        out_weight,
        preferred_element_type=jnp.float32,
    ).astype(jnp.bfloat16)
    partial_mix = lax.all_to_all(column_part, "ep", split_axis=0, concat_axis=1, tiled=True).astype(
        jnp.float32
    )
    mixed_sum = rounded(
        lax.psum(rounded(partial_mix).astype(jnp.bfloat16), "tp").astype(jnp.float32)
    )
    middle = rounded(tokens.astype(jnp.float32) + scaled_rows(mixed_sum, post_gain))
    moe_in = scaled_rows(middle, ffn_gain).astype(jnp.bfloat16)
    experts_all = lax.axis_size("ep")
    topk_here = routes.shape[1]
    capacity = seq_here * topk_here // experts_all + 2
    slot_count = experts_all * capacity
    flat_routes = routes.reshape(-1)
    onehot = (flat_routes[:, None] == jnp.arange(experts_all, dtype=jnp.int32)[None, :]).astype(
        jnp.int32
    )
    earlier = jnp.cumsum(onehot, axis=0) - onehot
    ranks = jnp.sum(earlier * onehot, axis=1)
    slot_ids = flat_routes * capacity + ranks
    placing = (jnp.arange(slot_count, dtype=jnp.int32)[:, None] == slot_ids[None, :]).reshape(
        slot_count, seq_here, topk_here
    )
    dispatch_rows = jnp.any(placing, axis=2).astype(jnp.bfloat16)
    combine = jnp.sum(
        jnp.where(placing, route_gates[None, :, :], jnp.zeros((), jnp.float32)), axis=2
    ).T
    outgoing = jnp.dot(dispatch_rows, moe_in, preferred_element_type=jnp.float32).astype(
        jnp.bfloat16
    )
    outgoing = outgoing.reshape(experts_all, capacity, model_width)
    gate_local = expert_gate[0]
    up_local = expert_up[0]
    down_local = expert_down[0]
    arrived = lax.all_to_all(outgoing, "ep", split_axis=0, concat_axis=0, tiled=True)
    sources = arrived.shape[0]
    held_slots = arrived.shape[1]
    flat_in = arrived.reshape(sources * held_slots, model_width)
    hidden = (
        jax.nn.silu(jnp.dot(flat_in, gate_local, preferred_element_type=jnp.float32))
        * jnp.dot(flat_in, up_local, preferred_element_type=jnp.float32)
    ).astype(jnp.bfloat16)
    partial_out = rounded(jnp.dot(hidden, down_local, preferred_element_type=jnp.float32))
    expert_sum = lax.psum(partial_out.astype(jnp.bfloat16), "tp")
    returned = lax.all_to_all(
        expert_sum.reshape(sources, held_slots, -1), "ep", split_axis=0, concat_axis=0, tiled=True
    )
    back_rows = returned.reshape(slot_count, -1).astype(jnp.float32)
    routed = jnp.dot(combine, back_rows, precision=lax.Precision.HIGHEST)
    shared_hidden = (
        jax.nn.silu(jnp.dot(moe_in, shared_gate, preferred_element_type=jnp.float32))
        * jnp.dot(moe_in, shared_up, preferred_element_type=jnp.float32)
    ).astype(jnp.bfloat16)
    shared_part = rounded(jnp.dot(shared_hidden, shared_down, preferred_element_type=jnp.float32))
    shared_out = lax.psum(shared_part.astype(jnp.bfloat16), "tp")
    mixture = shared_out.astype(jnp.float32) + routed
    result = (middle + scaled_rows(mixture, out_gain)).astype(jnp.bfloat16)
    return (result, new_state)


def solution(mesh):
    return jax.shard_map(
        on_device,
        mesh=mesh,
        in_specs=(
            P("ep", None),
            P("ep"),
            P("ep", "tp", None, None),
            P(),
            P(),
            P(),
            P(),
            P("ep", "tp"),
            P("ep", "tp"),
            P("ep", "tp"),
            P("ep", "tp"),
            P("tp", "ep"),
            P("ep", None),
            P("ep", None),
            P("ep", None, "tp"),
            P("ep", None, "tp"),
            P("ep", "tp", None),
            P(None, "tp"),
            P(None, "tp"),
            P("tp", None),
        ),
        out_specs=(P("ep", None), P("ep", "tp", None, None)),
        check_vma=False,
    )
```

profile of v0, /device:TPU:0, one launch (start us, length us, event | category | flops | bytes accessed | tf_op | source)
XLA Modules:
  0.0 254.3 jit_solution(6704595756294250518)
XLA Ops:
  7.2 1.0 fusion.25
  8.3 0.9 copy_bitcast_fusion.1
  9.2 15.7 %all_to_all.48 = bf16[16,16,128]{2,0,1:T(8,128)(2,1)S(1)} all-to-all(bf16[16,16,128]{2,0,1:T(8,128)(2,1)S(1)} %copy_bitcast_fusion.1), channel_id=1, replica_groups=mesh['ep'=16,'tp'=2] {'ep'}, dimensions={1} | all-to-all | bytes 131072 | tf_op jit(solution)/shard_map/all_to_all | solution.py:88
  24.9 2.8 %fusion.11 = f32[256,2048]{1,0:T(8,128)} fusion(bf16[256,128]{1,0:T(8,128)(2,1)S(1)} %bitcast.57, bf16[128,512]{1,0:T(8,128)(2,1)} %param.30, bf16[128,512]{1,0:T(8,128)(2,1)} %param.29, bf16[128,512]{1,0:T(8,128)(2,1)} %param.28, bf16[128,512]{1,0:T(8,128)(2,1)} %param.27), kind=kOutput, calls=%fused_computation.18 | convolution fusion | flops 136314880 | bytes 2686976 | tf_op jit(solution)/shard_map/dot_general | solution.py:91
  28.1 0.1 reduce_window_sum.11
  28.2 0.2 select_reduce_fusion.1
  28.8 77.1 %reduce-scatter.2.cloned.1.call-done = f32[16,2048]{1,0:T(8,128)} async-done(((f32[256,2048]{1,0:T(8,128)}), f32[16,2048]{1,0:T(8,128)}) %reduce-scatter.2.cloned.1.call-update) | async-done | bytes 131088 | tf_op jit(solution)/shard_map/reduce_scatter | solution.py:90
  105.9 0.9 convert.9
  107.3 5.3 %fusion.62 = f32[16,8,1,64]{3,2,1,0:T(1,128)S(1)} fusion(f32[16,8,64,1]{2,3,1,0:T(1,128)S(1)} %bitcast.55, f32[16,8,64,64]{3,2,1,0:T(8,128)} %param.22), kind=kOutput, calls=%fused_computation.103 | convolution fusion | flops 6291456 | bytes 2162688 | tf_op jit(solution)/shard_map/shd,shde->she/dot_general | solution.py:46
  112.6 0.2 multiply_reduce_fusion.1
  113.0 38.2 %all_gather.3 = bf16[256,512]{1,0:T(8,128)(2,1)S(1)} all-gather(bf16[16,512]{1,0:T(8,128)(2,1)S(1)} %fusion.46), channel_id=1, replica_groups=mesh['ep'=16,'tp'=2] {'ep'}, dimensions={0}, use_global_device_ids=true | all-gather | bytes 278528 | tf_op jit(solution)/shard_map/all_gather | solution.py:106
  151.2 0.8 convolution_convert_fusion.3
  152.1 3.5 %all-to-all-start.1 = ((bf16[16,16,128]{2,1,0:T(8,128)(2,1)}), bf16[16,16,128]{2,1,0:T(8,128)(2,1)S(1)}, u32[]{:S(2)}, u32[]{:S(2)}) async-start(bf16[16,16,128]{2,1,0:T(8,128)(2,1)} %bitcast.6), calls=%async_computation.2 | async-start | bytes 131072 | tf_op jit(solution)/shard_map/all_to_all | solution.py:110
  155.6 7.4 %all-to-all-done.1 = bf16[16,16,128]{2,1,0:T(8,128)(2,1)S(1)} async-done(((bf16[16,16,128]{2,1,0:T(8,128)(2,1)}), bf16[16,16,128]{2,1,0:T(8,128)(2,1)S(1)}, u32[]{:S(2)}, u32[]{:S(2)}) %all-to-all-start.1) | async-done | bytes 65568 | tf_op jit(solution)/shard_map/all_to_all | solution.py:110
  163.1 0.6 copy_bitcast_fusion
  163.8 14.5 %all-reduce.4.cloned.1.call-done = bf16[16,2048]{1,0:T(8,128)(2,1)} async-done(((bf16[16,2048]{1,0:T(8,128)(2,1)}), bf16[16,2048]{1,0:T(8,128)(2,1)}) %all-reduce.4.cloned.1.call-update) | async-done | bytes 65552 | tf_op jit(solution)/shard_map/psum | solution.py:114
  178.3 1.0 fusion.23
  179.3 0.9 fusion.28
  180.2 0.1 fusion.29
  180.4 1.1 fusion.1
  181.5 6.8 %all-to-all-start.2 = ((bf16[16,8,2048]{2,1,0:T(8,128)(2,1)}), bf16[16,8,2048]{2,1,0:T(8,128)(2,1)S(1)}, u32[]{:S(2)}, u32[]{:S(2)}) async-start(bf16[16,8,2048]{2,1,0:T(8,128)(2,1)} %fusion.1), calls=%async_computation.3 | async-start | bytes 1048576 | tf_op jit(solution)/shard_map/all_to_all | solution.py:143
  188.4 1.5 fusion.60
  189.9 3.0 %convolution_convert_fusion.2 = bf16[16,2048]{1,0:T(8,128)(2,1)} fusion(bf16[256,2048]{1,0:T(8,128)(2,1)} %param.39, bf16[2048,256]{1,0:T(8,128)(2,1)} %param.38, f32[16,256]{1,0:T(8,128)S(1)} %fusion.60, bf16[16,2048]{1,0:T(8,128)(2,1)S(1)} %fusion.28, f32[2048]{0:T(1024)S(1)} %copy-done.4, f32[16]{0:T(128)S(1)} %add_rsqrt_fusion.2), kind=kOutput, calls=%fused_computation.6 | convolution fusion | flops 33742848 | bytes 2252864 | tf_op jit(solution)/shard_map/dot_general | solution.py:162
  192.9 10.9 %all-to-all-done.2 = bf16[16,8,2048]{2,1,0:T(8,128)(2,1)S(1)} async-done(((bf16[16,8,2048]{2,1,0:T(8,128)(2,1)}), bf16[16,8,2048]{2,1,0:T(8,128)(2,1)S(1)}, u32[]{:S(2)}, u32[]{:S(2)}) %all-to-all-start.2) | async-done | bytes 524320 | tf_op jit(solution)/shard_map/all_to_all | solution.py:143
  203.8 1.5 fusion.9
  205.4 1.6 convolution_convert_fusion
  207.0 17.3 %all-reduce.6.cloned.1.call-done = (bf16[16,8,2048]{2,1,0:T(8,128)(2,1)}, bf16[16,2048]{1,0:T(8,128)(2,1)}) async-done(((bf16[16,8,2048]{2,1,0:T(8,128)(2,1)}, bf16[16,2048]{1,0:T(8,128)(2,1)}), (bf16[16,8,2048]{2,1,0:T(8,128)(2,1)}, bf16[16,2048]{1,0:T(8,128)(2,1)})) %all-reduce.6.cloned.1.call-update) | async-done | bytes 589840 | tf_op jit(solution)/shard_map/psum | solution.py:152
  224.3 6.8 %all-to-all-start.3 = ((bf16[16,8,2048]{2,1,0:T(8,128)(2,1)}), bf16[16,8,2048]{2,1,0:T(8,128)(2,1)S(1)}, u32[]{:S(2)}, u32[]{:S(2)}) async-start(bf16[16,8,2048]{2,1,0:T(8,128)(2,1)} %get-tuple-element.2), calls=%async_computation.4 | async-start | bytes 1048576 | tf_op jit(solution)/shard_map/all_to_all | solution.py:153
  231.2 4.3 %multiply_add_fusion = f32[16,8,64,64]{3,2,1,0:T(8,128)} fusion(f32[16,8,64,64]{3,2,1,0:T(8,128)} %param.22, f32[16,8,64]{2,1,0:T(8,128)S(1)} %reshape.193, f32[16,8,64]{2,1,0:T(8,128)S(1)} %get-tuple-element.20, f32[8]{0:T(128)S(1)} %dynamic_slice.3), kind=kLoop, calls=%fused_computation.1 | loop fusion | flops 1572864 | bytes 4259872 | tf_op jit(solution)/shard_map/add | solution.py:52
  235.5 11.1 %all-to-all-done.3 = bf16[16,8,2048]{2,1,0:T(8,128)(2,1)S(1)} async-done(((bf16[16,8,2048]{2,1,0:T(8,128)(2,1)}), bf16[16,8,2048]{2,1,0:T(8,128)(2,1)S(1)}, u32[]{:S(2)}, u32[]{:S(2)}) %all-to-all-start.3) | async-done | bytes 524320 | tf_op jit(solution)/shard_map/all_to_all | solution.py:153
  246.6 0.4 multiply_reduce_fusion
  247.0 0.7 fusion.32
  (55 shorter events, 1.7 us)
Async XLA Ops:
  7.2 198.2 %copy-start = (bf16[1,256,2048]{2,1,0:T(8,128)(2,1)S(1)}, bf16[1,256,2048]{2,1,0:T(8,128)(2,1)}, u32[]{:S(2)}) copy-start(bf16[1,256,2048]{2,1,0:T(8,128)(2,1)} %param.36) | copy-start | bytes 3145732
  7.2 20.6 %copy-start.10 = (s32[16]{0:T(128)S(1)}, s32[16]{0:T(128)}, u32[]{:S(2)}) copy-start(s32[16]{0:T(128)} %param.21) | copy-start | bytes 196
  7.2 20.6 %copy-start.6 = (s32[16,6]{0,1:T(8,128)S(1)}, s32[16,6]{0,1:T(8,128)}, u32[]{:S(2)}) copy-start(s32[16,6]{0,1:T(8,128)} %param.32) | copy-start | bytes 1156
  7.2 98.7 %reduce-scatter.2.cloned.1.call-start = ((), (), s32[]{:S(2)}) async-start(), calls=%async_computation.5 | async-start | bytes 2228224 | tf_op jit(solution)/shard_map/reduce_scatter | solution.py:90
  27.7 123.5 %copy-start.3 = (bf16[512,128]{1,0:T(8,128)(2,1)S(1)}, bf16[512,128]{1,0:T(8,128)(2,1)}, u32[]{:S(2)}) copy-start(bf16[512,128]{1,0:T(8,128)(2,1)} %param.31) | copy-start | bytes 393220
  27.8 151.5 %copy-start.2 = (bf16[16,2048]{1,0:T(8,128)(2,1)S(1)}, bf16[16,2048]{1,0:T(8,128)(2,1)}, u32[]{:S(2)}) copy-start(bf16[16,2048]{1,0:T(8,128)(2,1)} %param.20) | copy-start | bytes 196612
  27.8 151.5 %copy-start.7 = (f32[2048]{0:T(1024)S(1)}, f32[2048]{0:T(1024)}, u32[]{:S(2)}) copy-start(f32[2048]{0:T(1024)} %param.24) | copy-start | bytes 24580
  27.8 152.6 %copy-start.4 = (f32[2048]{0:T(1024)S(1)}, f32[2048]{0:T(1024)}, u32[]{:S(2)}) copy-start(f32[2048]{0:T(1024)} %param.25) | copy-start | bytes 24580
  112.9 92.5 %copy-start.1 = (bf16[1,2048,256]{2,1,0:T(8,128)(2,1)S(1)}, bf16[1,2048,256]{2,1,0:T(8,128)(2,1)}, u32[]{:S(2)}) copy-start(bf16[1,2048,256]{2,1,0:T(8,128)(2,1)} %param.35) | copy-start | bytes 3145732
  152.1 11.0 %all-to-all-start.1 = ((bf16[16,16,128]{2,1,0:T(8,128)(2,1)}), bf16[16,16,128]{2,1,0:T(8,128)(2,1)S(1)}, u32[]{:S(2)}, u32[]{:S(2)}) async-start(bf16[16,16,128]{2,1,0:T(8,128)(2,1)} %bitcast.6), calls=%async_computation.2 | async-start | bytes 131072 | tf_op jit(solution)/shard_map/all_to_all | solution.py:110
  155.6 22.7 %all-reduce.4.cloned.1.call-start = ((), (), s32[]{:S(2)}) async-start(), calls=%async_computation.6 | async-start | bytes 131072 | tf_op jit(solution)/shard_map/psum | solution.py:114
  181.5 22.3 %all-to-all-start.2 = ((bf16[16,8,2048]{2,1,0:T(8,128)(2,1)}), bf16[16,8,2048]{2,1,0:T(8,128)(2,1)S(1)}, u32[]{:S(2)}, u32[]{:S(2)}) async-start(bf16[16,8,2048]{2,1,0:T(8,128)(2,1)} %fusion.1), calls=%async_computation.3 | async-start | bytes 1048576 | tf_op jit(solution)/shard_map/all_to_all | solution.py:143
  188.4 35.9 %all-reduce.6.cloned.1.call-start = ((), (), s32[]{:S(2)}) async-start(), calls=%async_computation.7 | async-start | bytes 1179648 | tf_op jit(solution)/shard_map/psum | solution.py:152
  189.9 41.2 %copy-start.9 = (f32[16,6]{0,1:T(8,128)S(1)}, f32[16,6]{0,1:T(8,128)}, u32[]{:S(2)}) copy-start(f32[16,6]{0,1:T(8,128)} %param.33) | copy-start | bytes 1156
  224.3 22.3 %all-to-all-start.3 = ((bf16[16,8,2048]{2,1,0:T(8,128)(2,1)}), bf16[16,8,2048]{2,1,0:T(8,128)(2,1)S(1)}, u32[]{:S(2)}, u32[]{:S(2)}) async-start(bf16[16,8,2048]{2,1,0:T(8,128)(2,1)} %get-tuple-element.2), calls=%async_computation.4 | async-start | bytes 1048576 | tf_op jit(solution)/shard_map/all_to_all | solution.py:153
  231.2 15.4 %copy-start.5 = (bf16[16,2048]{1,0:T(8,128)(2,1)S(1)}, bf16[16,2048]{1,0:T(8,128)(2,1)}, u32[]{:S(2)}) copy-start(bf16[16,2048]{1,0:T(8,128)(2,1)} %get-tuple-element.3) | copy-start | bytes 196612
  231.2 15.8 %copy-start.8 = (f32[2048]{0:T(1024)S(1)}, f32[2048]{0:T(1024)}, u32[]{:S(2)}) copy-start(f32[2048]{0:T(1024)} %param.26) | copy-start | bytes 24580
Sparse Core Ops, SparseCore 0:
  27.9 77.9 reduce-scatter.1
  163.9 14.3 all-reduce.3
  207.1 17.0 all-reduce.5
where the time goes:
time: 255 us; the launch traced here: 254 us
  waiting for transfers between devices  138 us (54%)
  blocking collectives  53.9 us (21%)
  matrix products  18.1 us (7%)
  starting transfers between devices  17.3 us (7%)
  between operations  14.1 us (6%)
  other arithmetic  11.2 us (4%)
    reduce_scatter x1, waiting for transfers between devices, on_device(): lax.psum_scatter(jnp.dot(features, joined, preferred_element_type=jnp.flo...  77.1 us
    all_gather x1, blocking collectives, on_device(): lax.all_gather(retained, 'ep', axis=0, tiled=True)  38.2 us
    psum x1, waiting for transfers between devices, on_device(): expert_sum = lax.psum(partial_out.astype(jnp.bfloat16), 'tp')  17.3 us
    all_to_all x1, blocking collectives, on_device(): lax.all_to_all(normed, 'ep', split_axis=1, concat_axis=0, tiled=True)  15.7 us
    psum x1, waiting for transfers between devices, on_device(): lax.psum(rounded(partial_mix).astype(jnp.bfloat16), 'tp')  14.5 us
    all_to_all x1, waiting for transfers between devices, on_device(): lax.all_to_all(expert_sum.reshape(sources, held_slots, -1), 'ep', split_a...  11.1 us
    all_to_all x1, waiting for transfers between devices, on_device(): lax.all_to_all(outgoing, 'ep', split_axis=0, concat_axis=0, tiled=True)  10.9 us
    all_to_all x1, waiting for transfers between devices, on_device(): lax.all_to_all(column_part, 'ep', split_axis=0, concat_axis=1, tiled=True)  7.44 us
  transfers between devices with their start and end apart: 6, of which 6 were waited for; matrix products, arithmetic and copies ran while one was open for 4% of the time, Pallas kernels for 0%

commit v1 on v0

--- a/solution.py
+++ b/solution.py
@@ -85,7 +85,10 @@
     model_width = tokens.shape[1]
     local_cols = query_weight.shape[1]
     normed = scaled_rows(tokens, mix_gain).astype(jnp.bfloat16)
-    features = lax.all_to_all(normed, "ep", split_axis=1, concat_axis=0, tiled=True)
+    features = jnp.concatenate(
+        lax.all_to_all(jnp.stack(jnp.split(normed, lax.axis_size("ep"), axis=1)), "ep", 0, 0),
+        axis=0,
+    )
     joined = jnp.concatenate((query_weight, key_weight, value_weight, gate_weight), axis=1)
     summed = lax.psum_scatter(
         jnp.dot(features, joined, preferred_element_type=jnp.float32),

time: 255 us -> 255 us (level)
  no operation moved by 1% of the time
where the time goes in v1:
time: 255 us
  waiting for transfers between devices  138 us (54%)
  blocking collectives  53.9 us (21%)
  matrix products  18.1 us (7%)
  starting transfers between devices  17.3 us (7%)
  between operations  14.1 us (6%)
  other arithmetic  11.2 us (4%)
    reduce_scatter x1, waiting for transfers between devices, on_device(): lax.psum_scatter(jnp.dot(features, joined, preferred_element_type=jnp.flo...  77.1 us
    all_gather x1, blocking collectives, on_device(): lax.all_gather(retained, 'ep', axis=0, tiled=True)  38.2 us
    psum x1, waiting for transfers between devices, on_device(): expert_sum = lax.psum(partial_out.astype(jnp.bfloat16), 'tp')  17.3 us
    all_to_all x1, blocking collectives, on_device(): lax.all_to_all(jnp.stack(jnp.split(normed, lax.axis_size('ep'), axis=1)),...  15.7 us
    psum x1, waiting for transfers between devices, on_device(): lax.psum(rounded(partial_mix).astype(jnp.bfloat16), 'tp')  14.5 us
    all_to_all x1, waiting for transfers between devices, on_device(): lax.all_to_all(expert_sum.reshape(sources, held_slots, -1), 'ep', split_a...  11.1 us
    all_to_all x1, waiting for transfers between devices, on_device(): lax.all_to_all(outgoing, 'ep', split_axis=0, concat_axis=0, tiled=True)  10.9 us
    all_to_all x1, waiting for transfers between devices, on_device(): lax.all_to_all(column_part, 'ep', split_axis=0, concat_axis=1, tiled=True)  7.44 us
  transfers between devices with their start and end apart: 6, of which 6 were waited for; matrix products, arithmetic and copies ran while one was open for 4% of the time, Pallas kernels for 0%

profile of v1, /device:TPU:0, one launch (start us, length us, event | category | flops | bytes accessed | tf_op | source)
XLA Modules:
  0.0 254.6 jit_solution(13918871230000059889)
XLA Ops:
  7.2 1.0 fusion.25
  8.3 0.9 fusion.27
  9.4 15.7 %all_to_all.34 = bf16[16,16,128]{2,1,0:T(8,128)(2,1)S(1)} all-to-all(bf16[16,16,128]{2,1,0:T(8,128)(2,1)S(1)} %constant_dynamic-update-slice_fusion), channel_id=1, replica_groups=mesh['ep'=16,'tp'=2] {'ep'}, dimensions={0} | all-to-all | bytes 131072 | tf_op jit(solution)/shard_map/all_to_all | solution.py:89
  25.1 2.8 %fusion.11 = f32[256,2048]{1,0:T(8,128)} fusion(bf16[256,128]{1,0:T(8,128)(2,1)S(1)} %bitcast.114, bf16[128,512]{1,0:T(8,128)(2,1)} %param.30, bf16[128,512]{1,0:T(8,128)(2,1)} %param.29, bf16[128,512]{1,0:T(8,128)(2,1)} %param.28, bf16[128,512]{1,0:T(8,128)(2,1)} %param.27), kind=kOutput, calls=%fused_computation.18 | convolution fusion | flops 136314880 | bytes 2686976 | tf_op jit(solution)/shard_map/dot_general | solution.py:94
  28.3 0.1 reduce_window_sum.11
  28.5 0.2 select_reduce_fusion.1
  29.1 77.1 %reduce-scatter.2.cloned.1.call-done = f32[16,2048]{1,0:T(8,128)} async-done(((f32[256,2048]{1,0:T(8,128)}), f32[16,2048]{1,0:T(8,128)}) %reduce-scatter.2.cloned.1.call-update) | async-done | bytes 131088 | tf_op jit(solution)/shard_map/reduce_scatter | solution.py:93
  106.2 0.9 convert.9
  107.6 5.3 %fusion.61 = f32[16,8,1,64]{3,2,1,0:T(1,128)S(1)} fusion(f32[16,8,64,1]{2,3,1,0:T(1,128)S(1)} %bitcast.112, f32[16,8,64,64]{3,2,1,0:T(8,128)} %param.22), kind=kOutput, calls=%fused_computation.133 | convolution fusion | flops 6291456 | bytes 2162688 | tf_op jit(solution)/shard_map/shd,shde->she/dot_general | solution.py:46
  112.9 0.2 multiply_reduce_fusion.1
  113.3 38.2 %all_gather.3 = bf16[256,512]{1,0:T(8,128)(2,1)S(1)} all-gather(bf16[16,512]{1,0:T(8,128)(2,1)S(1)} %fusion.45), channel_id=1, replica_groups=mesh['ep'=16,'tp'=2] {'ep'}, dimensions={0}, use_global_device_ids=true | all-gather | bytes 278528 | tf_op jit(solution)/shard_map/all_gather | solution.py:109
  151.5 0.8 convolution_convert_fusion.3
  152.3 3.5 %all-to-all-start.1 = ((bf16[16,16,128]{2,1,0:T(8,128)(2,1)}), bf16[16,16,128]{2,1,0:T(8,128)(2,1)S(1)}, u32[]{:S(2)}, u32[]{:S(2)}) async-start(bf16[16,16,128]{2,1,0:T(8,128)(2,1)} %bitcast.21), calls=%async_computation.2 | async-start | bytes 131072 | tf_op jit(solution)/shard_map/all_to_all | solution.py:113
  155.9 7.4 %all-to-all-done.1 = bf16[16,16,128]{2,1,0:T(8,128)(2,1)S(1)} async-done(((bf16[16,16,128]{2,1,0:T(8,128)(2,1)}), bf16[16,16,128]{2,1,0:T(8,128)(2,1)S(1)}, u32[]{:S(2)}, u32[]{:S(2)}) %all-to-all-start.1) | async-done | bytes 65568 | tf_op jit(solution)/shard_map/all_to_all | solution.py:113
  163.3 0.6 copy_bitcast_fusion
  164.1 14.5 %all-reduce.4.cloned.1.call-done = bf16[16,2048]{1,0:T(8,128)(2,1)} async-done(((bf16[16,2048]{1,0:T(8,128)(2,1)}), bf16[16,2048]{1,0:T(8,128)(2,1)}) %all-reduce.4.cloned.1.call-update) | async-done | bytes 65552 | tf_op jit(solution)/shard_map/psum | solution.py:117
  178.6 1.0 fusion.23
  179.6 0.9 fusion.28
  180.5 0.1 fusion.29
  180.6 1.1 fusion.1
  181.8 6.8 %all-to-all-start.2 = ((bf16[16,8,2048]{2,1,0:T(8,128)(2,1)}), bf16[16,8,2048]{2,1,0:T(8,128)(2,1)S(1)}, u32[]{:S(2)}, u32[]{:S(2)}) async-start(bf16[16,8,2048]{2,1,0:T(8,128)(2,1)} %fusion.1), calls=%async_computation.3 | async-start | bytes 1048576 | tf_op jit(solution)/shard_map/all_to_all | solution.py:146
  188.7 1.5 fusion.59
  190.2 3.0 %convolution_convert_fusion.2 = bf16[16,2048]{1,0:T(8,128)(2,1)} fusion(bf16[256,2048]{1,0:T(8,128)(2,1)} %param.39, bf16[2048,256]{1,0:T(8,128)(2,1)} %param.38, f32[16,256]{1,0:T(8,128)S(1)} %fusion.59, bf16[16,2048]{1,0:T(8,128)(2,1)S(1)} %fusion.28, f32[2048]{0:T(1024)S(1)} %copy-done.4, f32[16]{0:T(128)S(1)} %add_rsqrt_fusion.2), kind=kOutput, calls=%fused_computation.6 | convolution fusion | flops 33742848 | bytes 2252864 | tf_op jit(solution)/shard_map/dot_general | solution.py:165
  193.2 10.9 %all-to-all-done.2 = bf16[16,8,2048]{2,1,0:T(8,128)(2,1)S(1)} async-done(((bf16[16,8,2048]{2,1,0:T(8,128)(2,1)}), bf16[16,8,2048]{2,1,0:T(8,128)(2,1)S(1)}, u32[]{:S(2)}, u32[]{:S(2)}) %all-to-all-start.2) | async-done | bytes 524320 | tf_op jit(solution)/shard_map/all_to_all | solution.py:146
  204.1 1.5 fusion.9
  205.7 1.6 convolution_convert_fusion
  207.3 17.3 %all-reduce.6.cloned.1.call-done = (bf16[16,8,2048]{2,1,0:T(8,128)(2,1)}, bf16[16,2048]{1,0:T(8,128)(2,1)}) async-done(((bf16[16,8,2048]{2,1,0:T(8,128)(2,1)}, bf16[16,2048]{1,0:T(8,128)(2,1)}), (bf16[16,8,2048]{2,1,0:T(8,128)(2,1)}, bf16[16,2048]{1,0:T(8,128)(2,1)})) %all-reduce.6.cloned.1.call-update) | async-done | bytes 589840 | tf_op jit(solution)/shard_map/psum | solution.py:155
  224.5 6.8 %all-to-all-start.3 = ((bf16[16,8,2048]{2,1,0:T(8,128)(2,1)}), bf16[16,8,2048]{2,1,0:T(8,128)(2,1)S(1)}, u32[]{:S(2)}, u32[]{:S(2)}) async-start(bf16[16,8,2048]{2,1,0:T(8,128)(2,1)} %get-tuple-element.2), calls=%async_computation.4 | async-start | bytes 1048576 | tf_op jit(solution)/shard_map/all_to_all | solution.py:156
  231.5 4.3 %multiply_add_fusion = f32[16,8,64,64]{3,2,1,0:T(8,128)} fusion(f32[16,8,64,64]{3,2,1,0:T(8,128)} %param.22, f32[16,8,64]{2,1,0:T(8,128)S(1)} %reshape.194, f32[16,8,64]{2,1,0:T(8,128)S(1)} %get-tuple-element.20, f32[8]{0:T(128)S(1)} %dynamic_slice.3), kind=kLoop, calls=%fused_computation.1 | loop fusion | flops 1572864 | bytes 4259872 | tf_op jit(solution)/shard_map/add | solution.py:52
  235.8 11.1 %all-to-all-done.3 = bf16[16,8,2048]{2,1,0:T(8,128)(2,1)S(1)} async-done(((bf16[16,8,2048]{2,1,0:T(8,128)(2,1)}), bf16[16,8,2048]{2,1,0:T(8,128)(2,1)S(1)}, u32[]{:S(2)}, u32[]{:S(2)}) %all-to-all-start.3) | async-done | bytes 524320 | tf_op jit(solution)/shard_map/all_to_all | solution.py:156
  246.9 0.4 multiply_reduce_fusion
  247.3 0.7 fusion.32
  (71 shorter events, 1.9 us)
Async XLA Ops:
  7.2 198.5 %copy-start = (bf16[1,256,2048]{2,1,0:T(8,128)(2,1)S(1)}, bf16[1,256,2048]{2,1,0:T(8,128)(2,1)}, u32[]{:S(2)}) copy-start(bf16[1,256,2048]{2,1,0:T(8,128)(2,1)} %param.36) | copy-start | bytes 3145732
  7.2 20.8 %copy-start.10 = (s32[16]{0:T(128)S(1)}, s32[16]{0:T(128)}, u32[]{:S(2)}) copy-start(s32[16]{0:T(128)} %param.21) | copy-start | bytes 196
  7.2 20.9 %copy-start.6 = (s32[16,6]{0,1:T(8,128)S(1)}, s32[16,6]{0,1:T(8,128)}, u32[]{:S(2)}) copy-start(s32[16,6]{0,1:T(8,128)} %param.32) | copy-start | bytes 1156
  7.2 99.0 %reduce-scatter.2.cloned.1.call-start = ((), (), s32[]{:S(2)}) async-start(), calls=%async_computation.5 | async-start | bytes 2228224 | tf_op jit(solution)/shard_map/reduce_scatter | solution.py:93
  28.0 123.5 %copy-start.3 = (bf16[512,128]{1,0:T(8,128)(2,1)S(1)}, bf16[512,128]{1,0:T(8,128)(2,1)}, u32[]{:S(2)}) copy-start(bf16[512,128]{1,0:T(8,128)(2,1)} %param.31) | copy-start | bytes 393220
  28.0 151.6 %copy-start.2 = (bf16[16,2048]{1,0:T(8,128)(2,1)S(1)}, bf16[16,2048]{1,0:T(8,128)(2,1)}, u32[]{:S(2)}) copy-start(bf16[16,2048]{1,0:T(8,128)(2,1)} %param.20) | copy-start | bytes 196612
  28.0 151.6 %copy-start.7 = (f32[2048]{0:T(1024)S(1)}, f32[2048]{0:T(1024)}, u32[]{:S(2)}) copy-start(f32[2048]{0:T(1024)} %param.24) | copy-start | bytes 24580
  28.0 152.6 %copy-start.4 = (f32[2048]{0:T(1024)S(1)}, f32[2048]{0:T(1024)}, u32[]{:S(2)}) copy-start(f32[2048]{0:T(1024)} %param.25) | copy-start | bytes 24580
  113.2 92.5 %copy-start.1 = (bf16[1,2048,256]{2,1,0:T(8,128)(2,1)S(1)}, bf16[1,2048,256]{2,1,0:T(8,128)(2,1)}, u32[]{:S(2)}) copy-start(bf16[1,2048,256]{2,1,0:T(8,128)(2,1)} %param.35) | copy-start | bytes 3145732
  152.3 11.0 %all-to-all-start.1 = ((bf16[16,16,128]{2,1,0:T(8,128)(2,1)}), bf16[16,16,128]{2,1,0:T(8,128)(2,1)S(1)}, u32[]{:S(2)}, u32[]{:S(2)}) async-start(bf16[16,16,128]{2,1,0:T(8,128)(2,1)} %bitcast.21), calls=%async_computation.2 | async-start | bytes 131072 | tf_op jit(solution)/shard_map/all_to_all | solution.py:113
  155.8 22.7 %all-reduce.4.cloned.1.call-start = ((), (), s32[]{:S(2)}) async-start(), calls=%async_computation.6 | async-start | bytes 131072 | tf_op jit(solution)/shard_map/psum | solution.py:117
  181.8 22.3 %all-to-all-start.2 = ((bf16[16,8,2048]{2,1,0:T(8,128)(2,1)}), bf16[16,8,2048]{2,1,0:T(8,128)(2,1)S(1)}, u32[]{:S(2)}, u32[]{:S(2)}) async-start(bf16[16,8,2048]{2,1,0:T(8,128)(2,1)} %fusion.1), calls=%async_computation.3 | async-start | bytes 1048576 | tf_op jit(solution)/shard_map/all_to_all | solution.py:146
  188.6 35.9 %all-reduce.6.cloned.1.call-start = ((), (), s32[]{:S(2)}) async-start(), calls=%async_computation.7 | async-start | bytes 1179648 | tf_op jit(solution)/shard_map/psum | solution.py:155
  190.2 41.2 %copy-start.9 = (f32[16,6]{0,1:T(8,128)S(1)}, f32[16,6]{0,1:T(8,128)}, u32[]{:S(2)}) copy-start(f32[16,6]{0,1:T(8,128)} %param.33) | copy-start | bytes 1156
  224.5 22.3 %all-to-all-start.3 = ((bf16[16,8,2048]{2,1,0:T(8,128)(2,1)}), bf16[16,8,2048]{2,1,0:T(8,128)(2,1)S(1)}, u32[]{:S(2)}, u32[]{:S(2)}) async-start(bf16[16,8,2048]{2,1,0:T(8,128)(2,1)} %get-tuple-element.2), calls=%async_computation.4 | async-start | bytes 1048576 | tf_op jit(solution)/shard_map/all_to_all | solution.py:156
  231.5 15.4 %copy-start.5 = (bf16[16,2048]{1,0:T(8,128)(2,1)S(1)}, bf16[16,2048]{1,0:T(8,128)(2,1)}, u32[]{:S(2)}) copy-start(bf16[16,2048]{1,0:T(8,128)(2,1)} %get-tuple-element.3) | copy-start | bytes 196612
  231.5 15.8 %copy-start.8 = (f32[2048]{0:T(1024)S(1)}, f32[2048]{0:T(1024)}, u32[]{:S(2)}) copy-start(f32[2048]{0:T(1024)} %param.26) | copy-start | bytes 24580
Sparse Core Ops, SparseCore 0:
  28.1 78.0 reduce-scatter.1
  164.1 14.3 all-reduce.3
  207.4 17.0 all-reduce.5
